TPU v7x, 512 devices: a whole 4x8x8 slice. The times are simulated.
512 devices in a mesh: tp: 64 (over z, y), dp: 8 (over x, core).
Axes of the slice: x: 4, y: 8, z: 8, core: 2. Of those that a mesh axis runs over, the one named last changes fastest.
Arguments:
- hidden: bfloat16 [64, 4096], P(None, 'dp'), may hold values from -6 to 6
- norm_gain: float32 [2, 4096], P(None, 'dp'), may hold values from 0.1 to 1.9
- gate_weight: bfloat16 [2, 4096, 8192], P(None, 'dp', 'tp'), may hold values from -0.09375 to 0.09375
- inner_weight: bfloat16 [2, 4096, 8192], P(None, 'dp', 'tp'), may hold values from -0.09375 to 0.09375
- write_weight: bfloat16 [2, 4096, 2048], P(None, 'dp', 'tp'), may hold values from -0.09375 to 0.09375
- read_weight: bfloat16 [2, 4096, 2048], P(None, 'dp', 'tp'), may hold values from -0.09375 to 0.09375
- step_weight: bfloat16 [2, 4096, 128], P(None, 'dp'), may hold values from -0.09375 to 0.09375
- conv_inner: bfloat16 [2, 4, 8192], P(None, None, 'tp'), may hold values from -3 to 3
- conv_write: bfloat16 [2, 4, 2048], P(None, None, 'tp'), may hold values from -3 to 3
- conv_read: bfloat16 [2, 4, 2048], P(None, None, 'tp'), may hold values from -3 to 3
- step_bias: float32 [2, 128], P(None, 'tp'), may hold values from -4 to -1
- decay_log: float32 [2, 128], P(None, 'tp'), may hold values from -3 to 0.5
- skip_gain: float32 [2, 128], P(None, 'tp'), may hold values from 0.1 to 1.9
- group_gain: float32 [2, 8192], P(None, 'tp'), may hold values from 0.1 to 1.9
- out_weight: bfloat16 [2, 8192, 4096], P(None, 'tp', 'dp'), may hold values from -0.4 to 0.4
- state_inner: bfloat16 [2, 64, 3, 8192], P(None, 'dp', None, 'tp'), may hold values from -6 to 6
- state_write: bfloat16 [2, 64, 3, 2048], P(None, 'dp', None, 'tp'), may hold values from -6 to 6
- state_read: bfloat16 [2, 64, 3, 2048], P(None, 'dp', None, 'tp'), may hold values from -6 to 6
- recurrent: float32 [2, 64, 128, 64, 128], P(None, 'dp', 'tp'), may hold values from -1.2 to 1.2, as said below
Outputs:
- out_hidden: bfloat16 [64, 4096], P(None, 'dp')
- next_inner: bfloat16 [2, 64, 3, 8192], P(None, 'dp', None, 'tp')
- next_write: bfloat16 [2, 64, 3, 2048], P(None, 'dp', None, 'tp')
- next_read: bfloat16 [2, 64, 3, 2048], P(None, 'dp', None, 'tp')
- next_recurrent: float32 [2, 64, 128, 64, 128], P(None, 'dp', 'tp')
Inputs may be any that keep to these rules, and one draw needn't show every extreme that they name: recurrent states of order a tenth, with scales that differ between heads.
All inputs are finite; a program needn't handle non-finite values.
Results may differ from a plain program's by a relative error of at most 0.025.
Values may be sent and summed in bfloat16 or wider, within the bound.
No kernel may reach another device: no remote copies, remote signals or barrier semaphores. Data moves between devices by JAX's collectives and lax.ppermute only.
A program may use at most 64 MiB of HBM per device.

v0:
```python
import jax
import jax.numpy as jnp
from jax import lax
from jax.sharding import Mesh
from jax.sharding import PartitionSpec as P

D = 4096
HEADS = 128
GROUPS = 16
DP = ("dp_0", "dp_1")
TP = ("tp_0", "tp_1")
TP_DP = ("tp_0", "tp_1", "dp_0", "dp_1")
eps = 1e-06


def cut_along(shard, dim, size):
    before, after = (shard.shape[:dim], shard.shape[dim + 1 :])
    return jnp.moveaxis(shard.reshape(*before, size, -1, *after), dim, 0)


def summed_on_arrival(shard, axis, dim):
    size = lax.axis_size(axis)
    pieces = lax.all_to_all(cut_along(shard, dim, size), axis, 0, 0, tiled=True)
    return jnp.sum(pieces.astype(jnp.float32), axis=0)


def side_by_side(arrays, axis, dim, along):
    widths = [a.shape[along] for a in arrays]
    both = jnp.concatenate(arrays, axis=along)
    result = summed_on_arrival(both, axis, dim)
    return tuple(jnp.split(result, [sum(widths[:k]) for k in range(1, len(widths))], axis=along))


def gather_turned(arrays, axis, dims):
    turned = [jnp.moveaxis(a, dim, 0) for a, dim in zip(arrays, dims)]
    both = jnp.concatenate([t.reshape(len(t), -1) for t in turned], axis=1)
    result, at, gathered = (lax.all_gather(both, axis, axis=0, tiled=True), 0, [])
    for t, dim in zip(turned, dims):
        share = result[:, at : at + t[0].size].reshape(-1, *t.shape[1:])
        gathered.append(jnp.moveaxis(share, 0, dim))
        at += t[0].size
    return tuple(gathered)


def over_axes(shard, axes):
    for axis in axes:
        shard = lax.psum(shard, axis)
    return shard


def copy_for_each(shard, axis):
    size = lax.axis_size(axis)
    return lax.all_to_all(
        jnp.broadcast_to(shard[None], (size, *shard.shape)), axis, 0, 0, tiled=True
    )


def laid_out(pieces, dim):
    lengths = list(pieces.shape[1:])
    lengths[dim] *= pieces.shape[0]
    return jnp.moveaxis(pieces, 0, dim).reshape(lengths)


def collect(shard, axis, dim):
    pieces = copy_for_each(shard, axis)
    return laid_out(pieces, dim)


def summed_on_arrival_2(shard, axis, dim):
    pieces = cut_along(shard, dim, lax.axis_size(axis))
    arrived = lax.all_to_all(pieces, axis, split_axis=0, concat_axis=0, tiled=True)
    return arrived.sum(axis=0)


def taken_together(shard, axis):
    return copy_for_each(shard, axis).sum(axis=0)


def convolve(state, fresh_row, kernel):
    window = jnp.concatenate([state, fresh_row[:, None, :]], axis=1)
    summed = jnp.sum(window.astype(jnp.float32) * kernel.astype(jnp.float32)[None], axis=1)
    return (jax.nn.silu(summed), window[:, 1:])


def mixer_block(normed, number, weights):
    (
        gate_weight,
        inner_weight,
        write_weight,
        read_weight,
        step_weight,
        conv_inner,
        conv_write,
        conv_read,
        step_bias,
        decay_log,
        skip_gain,
        group_gain,
        out_weight,
        state_inner,
        state_write,
        state_read,
        recurrent,
    ) = weights

    def partial_of(weight):
        return jnp.dot(normed, weight[number], preferred_element_type=jnp.float32).astype(
            jnp.bfloat16
        )

    summed = side_by_side(
        (
            partial_of(gate_weight),
            partial_of(inner_weight),
            partial_of(write_weight),
            partial_of(read_weight),
            partial_of(step_weight),
        ),
        DP,
        0,
        1,
    )
    gate_raw, inner_raw, write_raw, read_raw, step_raw = [
        member.astype(jnp.bfloat16) for member in summed
    ]
    inner_act, next_inner = convolve(state_inner[number], inner_raw, conv_inner[number])
    write_act, next_write = convolve(state_write[number], write_raw, conv_write[number])
    read_act, next_read = convolve(state_read[number], read_raw, conv_read[number])
    write_all, read_all = gather_turned(
        (write_act.astype(jnp.bfloat16), read_act.astype(jnp.bfloat16)), TP, (1, 1)
    )
    heads_here = step_bias.shape[1]
    head_dim = recurrent.shape[3]
    state_dim = recurrent.shape[4]
    rows_here = inner_act.shape[0]
    first_head = lax.axis_index(TP) * heads_here
    group_index = first_head // (HEADS // GROUPS)
    write_grid = write_all.reshape(rows_here, state_dim, GROUPS)
    read_grid = read_all.reshape(rows_here, state_dim, GROUPS)
    write_vec = lax.dynamic_slice_in_dim(write_grid, group_index, 1, 2)[:, :, 0].astype(jnp.float32)
    read_vec = lax.dynamic_slice_in_dim(read_grid, group_index, 1, 2)[:, :, 0].astype(jnp.float32)
    step_own = lax.dynamic_slice_in_dim(step_raw, first_head, heads_here, 1)
    step_size = jax.nn.softplus(step_own.astype(jnp.float32) + step_bias[number][None, :])
    retain = jnp.exp(-step_size * jnp.exp(decay_log[number])[None, :])
    inner_heads = inner_act.reshape(rows_here, heads_here, head_dim)
    updated = (
        retain[:, :, None, None] * recurrent[number]
        + (step_size[:, :, None] * inner_heads)[:, :, :, None] * write_vec[:, None, None, :]
    )
    readout = jnp.einsum("bhpn,bn->bhp", updated, read_vec, precision=lax.Precision.HIGHEST)
    readout = readout + skip_gain[number][None, :, None] * inner_heads
    gated_out = readout.reshape(rows_here, heads_here * head_dim) * jax.nn.silu(
        gate_raw.astype(jnp.float32)
    )
    selector = (jnp.arange(GROUPS) == group_index).astype(jnp.float32)
    totals = over_axes(jnp.sum(gated_out * gated_out, axis=1)[:, None] * selector[None, :], TP)
    group_sum = jnp.sum(totals * selector[None, :], axis=1, keepdims=True)
    group_factor = lax.rsqrt(group_sum / (HEADS // GROUPS * head_dim) + eps)
    group_normed = (gated_out * group_factor * group_gain[number][None, :]).astype(jnp.bfloat16)
    branch = jnp.dot(
        collect(group_normed, DP, 0), out_weight[number], preferred_element_type=jnp.float32
    )
    return (branch, (next_inner, next_write, next_read, updated))


def columns_over(branch):
    return summed_on_arrival_2(branch, TP, 1)


def local(
    hidden,
    norm_gain,
    gate_weight,
    inner_weight,
    write_weight,
    read_weight,
    step_weight,
    conv_inner,
    conv_write,
    conv_read,
    step_bias,
    decay_log,
    skip_gain,
    group_gain,
    out_weight,
    state_inner,
    state_write,
    state_read,
    recurrent,
):
    weights = (
        gate_weight,
        inner_weight,
        write_weight,
        read_weight,
        step_weight,
        conv_inner,
        conv_write,
        conv_read,
        step_bias,
        decay_log,
        skip_gain,
        group_gain,
        out_weight,
        state_inner,
        state_write,
        state_read,
        recurrent,
    )
    wide_in = hidden.astype(jnp.float32)
    squares = taken_together(jnp.sum(wide_in * wide_in, axis=1, keepdims=True), DP)
    normed = (wide_in * lax.rsqrt(squares / D + eps) * norm_gain[0][None, :]).astype(jnp.bfloat16)
    branch, first_states = mixer_block(normed, 0, weights)
    slice_width = hidden.shape[1] // lax.axis_size(TP)
    offset = lax.axis_index(TP) * slice_width
    own_cols = lax.dynamic_slice_in_dim(wide_in, offset, slice_width, 1)
    middle = (own_cols + columns_over(branch)).astype(jnp.bfloat16).astype(jnp.float32)
    squares = over_axes(jnp.sum(middle * middle, axis=1, keepdims=True), TP_DP)
    gain_slice = lax.dynamic_slice_in_dim(norm_gain[1], offset, slice_width, 0)
    normed_part = (middle * lax.rsqrt(squares / D + eps) * gain_slice[None, :]).astype(jnp.bfloat16)
    normed = collect(normed_part, TP, 1)
    branch, second_states = mixer_block(normed, 1, weights)
    result = collect((middle + columns_over(branch)).astype(jnp.bfloat16), TP, 1)
    stacked = [jnp.stack([earlier, later]) for earlier, later in zip(first_states, second_states)]
    return (result, stacked[0], stacked[1], stacked[2], stacked[3])


def solution(mesh):
    finer = Mesh(mesh.devices.reshape(8, 8, 4, 2), ("tp_0", "tp_1", "dp_0", "dp_1"))
    placed = (
        P(None, DP),
        P(None, DP),
        P(None, DP, TP),
        P(None, DP, TP),
        P(None, DP, TP),
        P(None, DP, TP),
        P(None, DP, None),
        P(None, None, TP),
        P(None, None, TP),
        P(None, None, TP),
        P(None, TP),
        P(None, TP),
        P(None, TP),
        P(None, TP),
        P(None, TP, DP),
        P(None, DP, None, TP),
        P(None, DP, None, TP),
        P(None, DP, None, TP),
        P(None, DP, TP, None, None),
    )
    return jax.shard_map(
        local,
        mesh=finer,
        in_specs=placed,
        out_specs=(
            P(None, DP),
            P(None, DP, None, TP),
            P(None, DP, None, TP),
            P(None, DP, None, TP),
            P(None, DP, TP, None, None),
        ),
        check_vma=False,
    )
```

profile of v0, /device:TPU:8, one launch (start us, length us, event | category | flops | bytes accessed | tf_op | source)
XLA Modules:
  0.0 351.3 jit_solution(7885808371134442058)
XLA Ops:
  0.6 1.0 copy.87
  1.7 0.6 broadcast_in_dim.24
  2.3 4.4 %all-to-all-start = ((f32[8,64,1]{1,2,0:T(1,128)}), f32[8,64,1]{1,2,0:T(1,128)S(1)}, u32[]{:S(2)}, u32[]{:S(2)}) async-start(f32[8,64,1]{1,2,0:T(1,128)} %broadcast_in_dim.24), calls=%async_computation | async-start | bytes 8192 | tf_op jit(solution)/shard_map/all_to_all | solution.py:53
  6.8 0.7 copy-done.12
  7.5 0.7 copy-done.13
  8.2 0.6 copy-done.8
  8.9 3.0 all-to-all-done
  12.0 0.3 convolution_convert_fusion.8
  12.4 0.4 copy-done.5
  12.8 0.3 convolution_convert_fusion.9
  13.2 0.3 convolution_convert_fusion.4
  13.5 0.5 copy-done.2
  14.0 0.3 convolution_convert_fusion.3
  14.3 0.6 copy-done.4
  14.9 0.3 convolution_convert_fusion.5
  15.3 0.7 concatenate.30
  16.0 3.4 all-to-all-start.1
  19.4 5.5 %all-to-all-done.1 = bf16[8,8,448]{2,1,0:T(8,128)(2,1)S(1)} async-done(((bf16[8,8,448]{2,1,0:T(8,128)(2,1)}), bf16[8,8,448]{2,1,0:T(8,128)(2,1)S(1)}, u32[]{:S(2)}, u32[]{:S(2)}) %all-to-all-start.1) | async-done | bytes 57376 | tf_op jit(solution)/shard_map/all_to_all | solution.py:23
  25.2 56.1 %all-gather = bf16[64,32,16]{1,2,0:T(8,128)(2,1)S(1)} all-gather(bf16[1,32,16]{1,2,0:T(8,128)(2,1)S(1)} %maximum_bitcast_fusion), channel_id=1, replica_groups=mesh['tp_0'=8,'tp_1'=8,'dp_0'=4,'dp_1'=2] {'tp_0','tp_1'}, dimensions={0}, use_global_device_ids=true | all-gather | bytes 66560 | tf_op jit(solution)/shard_map/all_gather | solution.py:37
  81.4 0.3 reshape.168
  82.3 0.3 dynamic-slice_reduce_fusion.1
  82.8 0.8 fusion.4
  84.0 16.0 %psum.56 = f32[8,16]{1,0:T(8,128)S(1)} all-reduce(f32[8,16]{1,0:T(8,128)S(1)} %broadcast_multiply_fusion.3), channel_id=1, replica_groups=mesh['tp_0'=8,'tp_1'=8,'dp_0'=4,'dp_1'=2] {'tp_0'}, use_global_device_ids=true, to_apply=%region_7.8 | all-reduce | flops 128 | bytes 1024 | tf_op jit(solution)/shard_map/psum | solution.py:47
  100.0 15.4 %psum.57 = f32[8,16]{1,0:T(8,128)S(1)} all-reduce(f32[8,16]{1,0:T(8,128)S(1)} %psum.56), channel_id=1, replica_groups=mesh['tp_0'=8,'tp_1'=8,'dp_0'=4,'dp_1'=2] {'tp_1'}, use_global_device_ids=true, to_apply=%region_8.9 | all-reduce | flops 128 | bytes 1024 | tf_op jit(solution)/shard_map/psum | solution.py:47
  115.6 0.6 broadcast_in_dim.28
  116.2 3.3 all-to-all-start.2
  119.7 5.1 %all-to-all-done.2 = bf16[8,8,128]{2,1,0:T(8,128)(2,1)S(1)} async-done(((bf16[8,8,128]{2,1,0:T(8,128)(2,1)}), bf16[8,8,128]{2,1,0:T(8,128)(2,1)S(1)}, u32[]{:S(2)}, u32[]{:S(2)}) %all-to-all-start.2) | async-done | bytes 16416 | tf_op jit(solution)/shard_map/all_to_all | solution.py:53
  125.2 0.8 reshape.185
  126.1 8.3 %all-to-all-start.3 = ((f32[64,1,512]{2,1,0:T(1,128)}), f32[64,1,512]{2,1,0:T(1,128)S(1)}, u32[]{:S(2)}, u32[]{:S(2)}) async-start(f32[64,1,512]{2,1,0:T(1,128)} %reshape.185), calls=%async_computation.3 | async-start | bytes 262144 | tf_op jit(solution)/shard_map/all_to_all | solution.py:71
  134.5 11.7 %all-to-all-done.3 = f32[64,1,512]{2,1,0:T(1,128)S(1)} async-done(((f32[64,1,512]{2,1,0:T(1,128)}), f32[64,1,512]{2,1,0:T(1,128)S(1)}, u32[]{:S(2)}, u32[]{:S(2)}) %all-to-all-start.3) | async-done | bytes 131104 | tf_op jit(solution)/shard_map/all_to_all | solution.py:71
  146.2 0.6 broadcast.160
  146.8 1.0 reduce.11
  148.0 14.8 %psum.58 = f32[64,1]{0,1:T(1,128)S(1)} all-reduce(f32[64,1]{0,1:T(1,128)S(1)} %bitcast.277), channel_id=1, replica_groups=mesh['tp_0'=8,'tp_1'=8,'dp_0'=4,'dp_1'=2] {'tp_0'}, use_global_device_ids=true, to_apply=%region_12.13 | all-reduce | flops 64 | bytes 512 | tf_op jit(solution)/shard_map/psum | solution.py:47
  162.8 15.4 %psum.59 = f32[64,1]{0,1:T(1,128)S(1)} all-reduce(f32[64,1]{0,1:T(1,128)S(1)} %psum.58), channel_id=1, replica_groups=mesh['tp_0'=8,'tp_1'=8,'dp_0'=4,'dp_1'=2] {'tp_1'}, use_global_device_ids=true, to_apply=%region_13.14 | all-reduce | flops 64 | bytes 512 | tf_op jit(solution)/shard_map/psum | solution.py:47
  178.2 8.9 %psum.60 = f32[64,1]{0,1:T(1,128)S(1)} all-reduce(f32[64,1]{0,1:T(1,128)S(1)} %psum.59), channel_id=1, replica_groups=mesh['tp_0'=8,'tp_1'=8,'dp_0'=4,'dp_1'=2] {'dp_0'}, use_global_device_ids=true, to_apply=%region_14.15 | all-reduce | flops 64 | bytes 512 | tf_op jit(solution)/shard_map/psum | solution.py:47
  187.1 2.5 psum.61
  189.7 0.8 reshape.187
  190.4 7.7 %all-to-all-start.4 = ((bf16[64,2,256]{2,1,0:T(2,128)(2,1)}), bf16[64,2,256]{2,1,0:T(2,128)(2,1)S(1)}, u32[]{:S(2)}, u32[]{:S(2)}) async-start(bf16[64,2,256]{2,1,0:T(2,128)(2,1)} %reshape.187), calls=%async_computation.4 | async-start | bytes 131072 | tf_op jit(solution)/shard_map/all_to_all | solution.py:53
  198.3 11.2 %all-to-all-done.4 = bf16[64,2,256]{2,1,0:T(2,128)(2,1)S(1)} async-done(((bf16[64,2,256]{2,1,0:T(2,128)(2,1)}), bf16[64,2,256]{2,1,0:T(2,128)(2,1)S(1)}, u32[]{:S(2)}, u32[]{:S(2)}) %all-to-all-start.4) | async-done | bytes 65568 | tf_op jit(solution)/shard_map/all_to_all | solution.py:53
  210.8 0.7 concatenate.35
  211.5 3.4 all-to-all-start.5
  214.9 5.5 %all-to-all-done.5 = bf16[8,8,448]{2,1,0:T(8,128)(2,1)S(1)} async-done(((bf16[8,8,448]{2,1,0:T(8,128)(2,1)}), bf16[8,8,448]{2,1,0:T(8,128)(2,1)S(1)}, u32[]{:S(2)}, u32[]{:S(2)}) %all-to-all-start.5) | async-done | bytes 57376 | tf_op jit(solution)/shard_map/all_to_all | solution.py:23
  220.8 47.6 %all-gather.1 = bf16[64,32,16]{1,2,0:T(8,128)(2,1)S(1)} all-gather(bf16[1,32,16]{1,2,0:T(8,128)(2,1)S(1)} %maximum_bitcast_fusion.1), channel_id=1, replica_groups=mesh['tp_0'=8,'tp_1'=8,'dp_0'=4,'dp_1'=2] {'tp_0','tp_1'}, dimensions={0}, use_global_device_ids=true | all-gather | bytes 66560 | tf_op jit(solution)/shard_map/all_gather | solution.py:37
  268.4 0.3 reshape.170
  269.4 0.3 dynamic-slice_reduce_fusion
  269.9 0.8 fusion.1
  271.0 14.8 %psum.62 = f32[8,16]{1,0:T(8,128)S(1)} all-reduce(f32[8,16]{1,0:T(8,128)S(1)} %broadcast_multiply_fusion.2), channel_id=1, replica_groups=mesh['tp_0'=8,'tp_1'=8,'dp_0'=4,'dp_1'=2] {'tp_0'}, use_global_device_ids=true, to_apply=%region_21.22 | all-reduce | flops 128 | bytes 1024 | tf_op jit(solution)/shard_map/psum | solution.py:47
  285.8 16.7 %psum.63 = f32[8,16]{1,0:T(8,128)S(1)} all-reduce(f32[8,16]{1,0:T(8,128)S(1)} %psum.62), channel_id=1, replica_groups=mesh['tp_0'=8,'tp_1'=8,'dp_0'=4,'dp_1'=2] {'tp_1'}, use_global_device_ids=true, to_apply=%region_22.23 | all-reduce | flops 128 | bytes 1024 | tf_op jit(solution)/shard_map/psum | solution.py:47
  302.7 0.6 broadcast_in_dim.34
  303.4 3.5 %all-to-all-start.6 = ((bf16[8,8,128]{2,1,0:T(8,128)(2,1)}), bf16[8,8,128]{2,1,0:T(8,128)(2,1)S(1)}, u32[]{:S(2)}, u32[]{:S(2)}) async-start(bf16[8,8,128]{2,1,0:T(8,128)(2,1)} %broadcast_in_dim.34), calls=%async_computation.6 | async-start | bytes 32768 | tf_op jit(solution)/shard_map/all_to_all | solution.py:53
  306.9 0.6 pad_maximum_fusion.2
  307.5 0.6 pad_maximum_fusion.3
  308.1 0.6 pad_maximum_fusion.1
  308.7 3.3 all-to-all-done.6
  312.4 0.8 reshape.189
  313.2 6.4 %all-to-all-start.7 = ((f32[64,1,512]{2,1,0:T(1,128)}), f32[64,1,512]{2,1,0:T(1,128)S(1)}, u32[]{:S(2)}, u32[]{:S(2)}) async-start(f32[64,1,512]{2,1,0:T(1,128)} %reshape.189), calls=%async_computation.7 | async-start | bytes 262144 | tf_op jit(solution)/shard_map/all_to_all | solution.py:71
  319.6 0.4 multiply_add_fusion.1
  320.1 11.4 %all-to-all-done.7 = f32[64,1,512]{2,1,0:T(1,128)S(1)} async-done(((f32[64,1,512]{2,1,0:T(1,128)}), f32[64,1,512]{2,1,0:T(1,128)S(1)}, u32[]{:S(2)}, u32[]{:S(2)}) %all-to-all-start.7) | async-done | bytes 131104 | tf_op jit(solution)/shard_map/all_to_all | solution.py:71
  331.5 1.0 reduce.12
  332.7 0.8 reshape.191
  333.5 5.4 %all-to-all-start.8 = ((bf16[64,2,256]{2,1,0:T(2,128)(2,1)}), bf16[64,2,256]{2,1,0:T(2,128)(2,1)S(1)}, u32[]{:S(2)}, u32[]{:S(2)}) async-start(bf16[64,2,256]{2,1,0:T(2,128)(2,1)} %reshape.191), calls=%async_computation.8 | async-start | bytes 131072 | tf_op jit(solution)/shard_map/all_to_all | solution.py:53
  338.9 1.0 pad_maximum_fusion
  339.9 10.5 %all-to-all-done.8 = bf16[64,2,256]{2,1,0:T(2,128)(2,1)S(1)} async-done(((bf16[64,2,256]{2,1,0:T(2,128)(2,1)}), bf16[64,2,256]{2,1,0:T(2,128)(2,1)S(1)}, u32[]{:S(2)}, u32[]{:S(2)}) %all-to-all-start.8) | async-done | bytes 65568 | tf_op jit(solution)/shard_map/all_to_all | solution.py:53
  350.5 0.7 copy.102
  (129 shorter events, 7.1 us)
Async XLA Ops:
  2.3 4.4 %copy-start.14 = (f32[2,2]{1,0:T(2,128)S(1)}, f32[2,2]{1,0:T(2,128)}, u32[]{:S(2)}) copy-start(f32[2,2]{1,0:T(2,128)} %param.31) | copy-start | bytes 52
  2.3 4.5 %copy-start.10 = (f32[2,512]{1,0:T(2,128)S(1)}, f32[2,512]{1,0:T(2,128)}, u32[]{:S(2)}) copy-start(f32[2,512]{1,0:T(2,128)} %param.20) | copy-start | bytes 12292
  2.3 4.5 %copy-start.11 = (bf16[2,4,128]{2,1,0:T(4,128)(2,1)S(1)}, bf16[2,4,128]{2,1,0:T(4,128)(2,1)}, u32[]{:S(2)}) copy-start(bf16[2,4,128]{2,1,0:T(4,128)(2,1)} %param.26) | copy-start | bytes 6148
  2.3 9.6 %all-to-all-start = ((f32[8,64,1]{1,2,0:T(1,128)}), f32[8,64,1]{1,2,0:T(1,128)S(1)}, u32[]{:S(2)}, u32[]{:S(2)}) async-start(f32[8,64,1]{1,2,0:T(1,128)} %broadcast_in_dim.24), calls=%async_computation | async-start | bytes 8192 | tf_op jit(solution)/shard_map/all_to_all | solution.py:53
  6.7 1.4 copy-start.7
  6.8 0.7 copy-start.12
  7.5 0.7 copy-start.13
  8.2 0.7 copy-start.8
  8.2 0.7 copy-start.9
  8.2 0.7 copy-start.16
  8.2 0.7 copy-start.17
  8.2 0.7 copy-start.15
  8.2 3.8 %copy-start.6 = (bf16[2,512,32]{1,2,0:T(8,128)(2,1)S(1)}, bf16[2,512,32]{1,2,0:T(8,128)(2,1)}, u32[]{:S(2)}) copy-start(bf16[2,512,32]{1,2,0:T(8,128)(2,1)} %param.24) | copy-start | bytes 196612
  11.9 0.8 copy-start.5
  12.0 1.2 copy-start.3
  13.0 1.0 copy-start.2
  14.0 0.9 copy-start.4
  16.0 8.9 %all-to-all-start.1 = ((bf16[8,8,448]{2,1,0:T(8,128)(2,1)}), bf16[8,8,448]{2,1,0:T(8,128)(2,1)S(1)}, u32[]{:S(2)}, u32[]{:S(2)}) async-start(bf16[8,8,448]{2,1,0:T(8,128)(2,1)} %bitcast.6), calls=%async_computation.1 | async-start | bytes 131072 | tf_op jit(solution)/shard_map/all_to_all | solution.py:23
  81.3 1.5 copy-start
  82.8 36.8 %copy-start.1 = (bf16[2,128,512]{2,1,0:T(8,128)(2,1)S(1)}, bf16[2,128,512]{2,1,0:T(8,128)(2,1)}, u32[]{:S(2)}) copy-start(bf16[2,128,512]{2,1,0:T(8,128)(2,1)} %param.33) | copy-start | bytes 786436
  116.2 8.6 %all-to-all-start.2 = ((bf16[8,8,128]{2,1,0:T(8,128)(2,1)}), bf16[8,8,128]{2,1,0:T(8,128)(2,1)S(1)}, u32[]{:S(2)}, u32[]{:S(2)}) async-start(bf16[8,8,128]{2,1,0:T(8,128)(2,1)} %broadcast_in_dim.28), calls=%async_computation.2 | async-start | bytes 32768 | tf_op jit(solution)/shard_map/all_to_all | solution.py:53
  126.1 20.2 %all-to-all-start.3 = ((f32[64,1,512]{2,1,0:T(1,128)}), f32[64,1,512]{2,1,0:T(1,128)S(1)}, u32[]{:S(2)}, u32[]{:S(2)}) async-start(f32[64,1,512]{2,1,0:T(1,128)} %reshape.185), calls=%async_computation.3 | async-start | bytes 262144 | tf_op jit(solution)/shard_map/all_to_all | solution.py:71
  190.4 19.0 %all-to-all-start.4 = ((bf16[64,2,256]{2,1,0:T(2,128)(2,1)}), bf16[64,2,256]{2,1,0:T(2,128)(2,1)S(1)}, u32[]{:S(2)}, u32[]{:S(2)}) async-start(bf16[64,2,256]{2,1,0:T(2,128)(2,1)} %reshape.187), calls=%async_computation.4 | async-start | bytes 131072 | tf_op jit(solution)/shard_map/all_to_all | solution.py:53
  211.5 8.9 %all-to-all-start.5 = ((bf16[8,8,448]{2,1,0:T(8,128)(2,1)}), bf16[8,8,448]{2,1,0:T(8,128)(2,1)S(1)}, u32[]{:S(2)}, u32[]{:S(2)}) async-start(bf16[8,8,448]{2,1,0:T(8,128)(2,1)} %bitcast.45), calls=%async_computation.5 | async-start | bytes 131072 | tf_op jit(solution)/shard_map/all_to_all | solution.py:23
  303.4 8.6 %all-to-all-start.6 = ((bf16[8,8,128]{2,1,0:T(8,128)(2,1)}), bf16[8,8,128]{2,1,0:T(8,128)(2,1)S(1)}, u32[]{:S(2)}, u32[]{:S(2)}) async-start(bf16[8,8,128]{2,1,0:T(8,128)(2,1)} %broadcast_in_dim.34), calls=%async_computation.6 | async-start | bytes 32768 | tf_op jit(solution)/shard_map/all_to_all | solution.py:53
  313.2 18.3 %all-to-all-start.7 = ((f32[64,1,512]{2,1,0:T(1,128)}), f32[64,1,512]{2,1,0:T(1,128)S(1)}, u32[]{:S(2)}, u32[]{:S(2)}) async-start(f32[64,1,512]{2,1,0:T(1,128)} %reshape.189), calls=%async_computation.7 | async-start | bytes 262144 | tf_op jit(solution)/shard_map/all_to_all | solution.py:71
  333.5 16.9 %all-to-all-start.8 = ((bf16[64,2,256]{2,1,0:T(2,128)(2,1)}), bf16[64,2,256]{2,1,0:T(2,128)(2,1)S(1)}, u32[]{:S(2)}, u32[]{:S(2)}) async-start(bf16[64,2,256]{2,1,0:T(2,128)(2,1)} %reshape.191), calls=%async_computation.8 | async-start | bytes 131072 | tf_op jit(solution)/shard_map/all_to_all | solution.py:53
where the time goes:
time: 352 us; the launch traced here: 351 us
  blocking collectives  208 us (59%)
  waiting for transfers between devices  67.3 us (19%)
  starting transfers between devices  45.8 us (13%)
  local copies, waits for them, and re-layouts  16.8 us (5%)
  other arithmetic  7.6 us (2%)
  matrix products  4.45 us (1%)
    psum x8, blocking collectives, over_axes(): shard = lax.psum(shard, axis)  104 us
    all_gather x2, blocking collectives, gather_turned(): lax.all_gather(both, axis, axis=0, tiled=True)  104 us
    all_to_all x5, waiting for transfers between devices, copy_for_each(): lax.all_to_all(jnp.broadcast_to(shard[None], (size, *shard.shape)), axis,...  33 us
    all_to_all x5, starting transfers between devices, copy_for_each(): lax.all_to_all(jnp.broadcast_to(shard[None], (size, *shard.shape)), axis,...  24.4 us
    all_to_all x2, waiting for transfers between devices, summed_on_arrival_2(): lax.all_to_all(pieces, axis, split_axis=0, concat_axis=0, tiled=True)  23.2 us
    all_to_all x2, starting transfers between devices, summed_on_arrival_2(): lax.all_to_all(pieces, axis, split_axis=0, concat_axis=0, tiled=True)  14.7 us
    all_to_all x2, waiting for transfers between devices, summed_on_arrival(): pieces = lax.all_to_all(cut_along(shard, dim, size), axis, 0, 0, tiled=True)  11.1 us
    unnamed x52, local copies, waits for them, and re-layouts  9.87 us
  transfers between devices with their start and end apart: 9, of which 9 were waited for; matrix products, arithmetic and copies ran while one was open for 1% of the time, Pallas kernels for 0%

commit v1 on v0

--- a/solution.py
+++ b/solution.py
@@ -34,7 +34,13 @@
 def gather_turned(arrays, axis, dims):
     turned = [jnp.moveaxis(a, dim, 0) for a, dim in zip(arrays, dims)]
     both = jnp.concatenate([t.reshape(len(t), -1) for t in turned], axis=1)
-    result, at, gathered = (lax.all_gather(both, axis, axis=0, tiled=True), 0, [])
+    result, at, gathered = (
+        jnp.concatenate(
+            lax.all_to_all(jnp.stack([both] * lax.axis_size(axis)), axis, 0, 0), axis=0
+        ),
+        0,
+        [],
+    )
     for t, dim in zip(turned, dims):
         share = result[:, at : at + t[0].size].reshape(-1, *t.shape[1:])
         gathered.append(jnp.moveaxis(share, 0, dim))

time: 352 us -> 293 us (0.83)
  blocking collectives: 208 us -> 102 us
  waiting for transfers between devices: 67.3 us -> 89.9 us
  starting transfers between devices: 45.8 us -> 67.9 us
    all_gather x2 -> x0, blocking collectives: 104 us -> none  [gather_turned(): lax.all_gather(both, axis, axis=0, tiled=True)]
    all_to_all x0 -> x2, starting transfers between devices: none -> 22 us  [gather_turned(): lax.all_to_all(jnp.stack([both] * lax.axis_size(axis)), axis, 0, 0)]
    all_to_all x0 -> x2, waiting for transfers between devices: none -> 21.3 us  [gather_turned(): lax.all_to_all(jnp.stack([both] * lax.axis_size(axis)), axis, 0, 0)]
    unnamed x52 -> x56, local copies, waits for them, and re-layouts: 9.87 us -> 11.4 us
  transfers between devices with their start and end apart: 9 -> 11, of which waited for: 9 -> 11; matrix products, arithmetic and copies ran while one was open for 1% -> 1% of each run, Pallas kernels for 0% -> 0%
where the time goes in v1:
time: 293 us; the launch traced here: 292 us
  blocking collectives  102 us (35%)
  waiting for transfers between devices  89.9 us (31%)
  starting transfers between devices  67.9 us (23%)
  local copies, waits for them, and re-layouts  18.9 us (6%)
  other arithmetic  7.6 us (3%)
  matrix products  4.45 us (2%)
    psum x8, blocking collectives, over_axes(): shard = lax.psum(shard, axis)  102 us
    all_to_all x5, waiting for transfers between devices, copy_for_each(): lax.all_to_all(jnp.broadcast_to(shard[None], (size, *shard.shape)), axis,...  34.4 us
    all_to_all x5, starting transfers between devices, copy_for_each(): lax.all_to_all(jnp.broadcast_to(shard[None], (size, *shard.shape)), axis,...  24.2 us
    all_to_all x2, waiting for transfers between devices, summed_on_arrival_2(): lax.all_to_all(pieces, axis, split_axis=0, concat_axis=0, tiled=True)  23.2 us
    all_to_all x2, starting transfers between devices, gather_turned(): lax.all_to_all(jnp.stack([both] * lax.axis_size(axis)), axis, 0, 0)  22 us
    all_to_all x2, waiting for transfers between devices, gather_turned(): lax.all_to_all(jnp.stack([both] * lax.axis_size(axis)), axis, 0, 0)  21.3 us
    all_to_all x2, starting transfers between devices, summed_on_arrival_2(): lax.all_to_all(pieces, axis, split_axis=0, concat_axis=0, tiled=True)  15.1 us
    unnamed x56, local copies, waits for them, and re-layouts  11.4 us
  transfers between devices with their start and end apart: 11, of which 11 were waited for; matrix products, arithmetic and copies ran while one was open for 1% of the time, Pallas kernels for 0%

profile of v1, /device:TPU:8, one launch (start us, length us, event | category | flops | bytes accessed | tf_op | source)
XLA Modules:
  0.0 292.1 jit_solution(9148775763894044777)
XLA Ops:
  0.6 1.0 copy.84
  1.7 0.6 broadcast_in_dim.24
  2.3 4.4 %all-to-all-start = ((f32[8,64,1]{1,2,0:T(1,128)}), f32[8,64,1]{1,2,0:T(1,128)S(1)}, u32[]{:S(2)}, u32[]{:S(2)}) async-start(f32[8,64,1]{1,2,0:T(1,128)} %broadcast_in_dim.24), calls=%async_computation | async-start | bytes 8192 | tf_op jit(solution)/shard_map/all_to_all | solution.py:59
  6.8 0.7 copy-done.12
  7.5 0.7 copy-done.13
  8.2 0.6 copy-done.8
  8.9 3.0 %all-to-all-done = f32[8,64,1]{1,2,0:T(1,128)S(1)} async-done(((f32[8,64,1]{1,2,0:T(1,128)}), f32[8,64,1]{1,2,0:T(1,128)S(1)}, u32[]{:S(2)}, u32[]{:S(2)}) %all-to-all-start) | async-done | bytes 2080 | tf_op jit(solution)/shard_map/all_to_all | solution.py:59
  12.4 0.4 copy-done.5
  13.2 0.3 convolution_convert_fusion.4
  13.5 0.5 copy-done.2
  14.0 0.3 convolution_convert_fusion.3
  14.3 0.6 copy-done.4
  14.9 0.3 convolution_convert_fusion.5
  15.3 0.7 concatenate.30
  16.0 3.4 %all-to-all-start.1 = ((bf16[8,8,448]{2,1,0:T(8,128)(2,1)}), bf16[8,8,448]{2,1,0:T(8,128)(2,1)S(1)}, u32[]{:S(2)}, u32[]{:S(2)}) async-start(bf16[8,8,448]{2,1,0:T(8,128)(2,1)} %bitcast.6), calls=%async_computation.1 | async-start | bytes 131072 | tf_op jit(solution)/shard_map/all_to_all | solution.py:23
  19.4 5.5 %all-to-all-done.1 = bf16[8,8,448]{2,1,0:T(8,128)(2,1)S(1)} async-done(((bf16[8,8,448]{2,1,0:T(8,128)(2,1)}), bf16[8,8,448]{2,1,0:T(8,128)(2,1)S(1)}, u32[]{:S(2)}, u32[]{:S(2)}) %all-to-all-start.1) | async-done | bytes 57376 | tf_op jit(solution)/shard_map/all_to_all | solution.py:23
  25.3 0.8 reshape.193
  26.1 16.6 %all-to-all-start.2 = ((bf16[64,2,256]{2,1,0:T(2,128)(2,1)}), bf16[64,2,256]{2,1,0:T(2,128)(2,1)S(1)}, u32[]{:S(2)}, u32[]{:S(2)}) async-start(bf16[64,2,256]{2,1,0:T(2,128)(2,1)} %reshape.193), calls=%async_computation.2 | async-start | bytes 131072 | tf_op jit(solution)/shard_map/all_to_all | solution.py:39
  42.8 11.2 %all-to-all-done.2 = bf16[64,2,256]{2,1,0:T(2,128)(2,1)S(1)} async-done(((bf16[64,2,256]{2,1,0:T(2,128)(2,1)}), bf16[64,2,256]{2,1,0:T(2,128)(2,1)S(1)}, u32[]{:S(2)}, u32[]{:S(2)}) %all-to-all-start.2) | async-done | bytes 65568 | tf_op jit(solution)/shard_map/all_to_all | solution.py:39
  54.3 0.3 reshape.158
  55.6 0.8 fusion.4
  56.8 14.8 %psum.56 = f32[8,16]{1,0:T(8,128)S(1)} all-reduce(f32[8,16]{1,0:T(8,128)S(1)} %broadcast_multiply_fusion.3), channel_id=1, replica_groups=mesh['tp_0'=8,'tp_1'=8,'dp_0'=4,'dp_1'=2] {'tp_0'}, use_global_device_ids=true, to_apply=%region_7.8 | all-reduce | flops 128 | bytes 1024 | tf_op jit(solution)/shard_map/psum | solution.py:53
  71.5 15.4 %psum.57 = f32[8,16]{1,0:T(8,128)S(1)} all-reduce(f32[8,16]{1,0:T(8,128)S(1)} %psum.56), channel_id=1, replica_groups=mesh['tp_0'=8,'tp_1'=8,'dp_0'=4,'dp_1'=2] {'tp_1'}, use_global_device_ids=true, to_apply=%region_8.9 | all-reduce | flops 128 | bytes 1024 | tf_op jit(solution)/shard_map/psum | solution.py:53
  87.2 0.6 broadcast_in_dim.28
  87.8 3.3 %all-to-all-start.3 = ((bf16[8,8,128]{2,1,0:T(8,128)(2,1)}), bf16[8,8,128]{2,1,0:T(8,128)(2,1)S(1)}, u32[]{:S(2)}, u32[]{:S(2)}) async-start(bf16[8,8,128]{2,1,0:T(8,128)(2,1)} %broadcast_in_dim.28), calls=%async_computation.3 | async-start | bytes 32768 | tf_op jit(solution)/shard_map/all_to_all | solution.py:59
  91.3 5.1 %all-to-all-done.3 = bf16[8,8,128]{2,1,0:T(8,128)(2,1)S(1)} async-done(((bf16[8,8,128]{2,1,0:T(8,128)(2,1)}), bf16[8,8,128]{2,1,0:T(8,128)(2,1)S(1)}, u32[]{:S(2)}, u32[]{:S(2)}) %all-to-all-start.3) | async-done | bytes 16416 | tf_op jit(solution)/shard_map/all_to_all | solution.py:59
  96.8 0.8 reshape.195
  97.7 7.5 %all-to-all-start.4 = ((f32[64,1,512]{2,1,0:T(1,128)}), f32[64,1,512]{2,1,0:T(1,128)S(1)}, u32[]{:S(2)}, u32[]{:S(2)}) async-start(f32[64,1,512]{2,1,0:T(1,128)} %reshape.195), calls=%async_computation.4 | async-start | bytes 262144 | tf_op jit(solution)/shard_map/all_to_all | solution.py:77
  105.3 11.7 %all-to-all-done.4 = f32[64,1,512]{2,1,0:T(1,128)S(1)} async-done(((f32[64,1,512]{2,1,0:T(1,128)}), f32[64,1,512]{2,1,0:T(1,128)S(1)}, u32[]{:S(2)}, u32[]{:S(2)}) %all-to-all-start.4) | async-done | bytes 131104 | tf_op jit(solution)/shard_map/all_to_all | solution.py:77
  117.0 0.6 broadcast.164
  117.6 1.0 reduce.11
  118.8 14.8 %psum.58 = f32[64,1]{0,1:T(1,128)S(1)} all-reduce(f32[64,1]{0,1:T(1,128)S(1)} %bitcast.281), channel_id=1, replica_groups=mesh['tp_0'=8,'tp_1'=8,'dp_0'=4,'dp_1'=2] {'tp_0'}, use_global_device_ids=true, to_apply=%region_12.13 | all-reduce | flops 64 | bytes 512 | tf_op jit(solution)/shard_map/psum | solution.py:53
  133.6 15.4 %psum.59 = f32[64,1]{0,1:T(1,128)S(1)} all-reduce(f32[64,1]{0,1:T(1,128)S(1)} %psum.58), channel_id=1, replica_groups=mesh['tp_0'=8,'tp_1'=8,'dp_0'=4,'dp_1'=2] {'tp_1'}, use_global_device_ids=true, to_apply=%region_13.14 | all-reduce | flops 64 | bytes 512 | tf_op jit(solution)/shard_map/psum | solution.py:53
  149.0 8.9 %psum.60 = f32[64,1]{0,1:T(1,128)S(1)} all-reduce(f32[64,1]{0,1:T(1,128)S(1)} %psum.59), channel_id=1, replica_groups=mesh['tp_0'=8,'tp_1'=8,'dp_0'=4,'dp_1'=2] {'dp_0'}, use_global_device_ids=true, to_apply=%region_14.15 | all-reduce | flops 64 | bytes 512 | tf_op jit(solution)/shard_map/psum | solution.py:53
  157.9 2.5 psum.61
  160.5 0.8 reshape.197
  161.3 7.7 %all-to-all-start.5 = ((bf16[64,2,256]{2,1,0:T(2,128)(2,1)}), bf16[64,2,256]{2,1,0:T(2,128)(2,1)S(1)}, u32[]{:S(2)}, u32[]{:S(2)}) async-start(bf16[64,2,256]{2,1,0:T(2,128)(2,1)} %reshape.197), calls=%async_computation.5 | async-start | bytes 131072 | tf_op jit(solution)/shard_map/all_to_all | solution.py:59
  169.1 11.2 %all-to-all-done.5 = bf16[64,2,256]{2,1,0:T(2,128)(2,1)S(1)} async-done(((bf16[64,2,256]{2,1,0:T(2,128)(2,1)}), bf16[64,2,256]{2,1,0:T(2,128)(2,1)S(1)}, u32[]{:S(2)}, u32[]{:S(2)}) %all-to-all-start.5) | async-done | bytes 65568 | tf_op jit(solution)/shard_map/all_to_all | solution.py:59
  181.6 0.7 concatenate.35
  182.3 3.4 %all-to-all-start.6 = ((bf16[8,8,448]{2,1,0:T(8,128)(2,1)}), bf16[8,8,448]{2,1,0:T(8,128)(2,1)S(1)}, u32[]{:S(2)}, u32[]{:S(2)}) async-start(bf16[8,8,448]{2,1,0:T(8,128)(2,1)} %bitcast.44), calls=%async_computation.6 | async-start | bytes 131072 | tf_op jit(solution)/shard_map/all_to_all | solution.py:23
  185.7 5.5 %all-to-all-done.6 = bf16[8,8,448]{2,1,0:T(8,128)(2,1)S(1)} async-done(((bf16[8,8,448]{2,1,0:T(8,128)(2,1)}), bf16[8,8,448]{2,1,0:T(8,128)(2,1)S(1)}, u32[]{:S(2)}, u32[]{:S(2)}) %all-to-all-start.6) | async-done | bytes 57376 | tf_op jit(solution)/shard_map/all_to_all | solution.py:23
  191.6 0.8 reshape.199
  192.4 5.4 %all-to-all-start.7 = ((bf16[64,2,256]{2,1,0:T(2,128)(2,1)}), bf16[64,2,256]{2,1,0:T(2,128)(2,1)S(1)}, u32[]{:S(2)}, u32[]{:S(2)}) async-start(bf16[64,2,256]{2,1,0:T(2,128)(2,1)} %reshape.199), calls=%async_computation.7 | async-start | bytes 131072 | tf_op jit(solution)/shard_map/all_to_all | solution.py:39
  197.8 0.6 pad_maximum_fusion.2
  198.6 0.6 pad_maximum_fusion.3
  199.2 10.0 %all-to-all-done.7 = bf16[64,2,256]{2,1,0:T(2,128)(2,1)S(1)} async-done(((bf16[64,2,256]{2,1,0:T(2,128)(2,1)}), bf16[64,2,256]{2,1,0:T(2,128)(2,1)S(1)}, u32[]{:S(2)}, u32[]{:S(2)}) %all-to-all-start.7) | async-done | bytes 65568 | tf_op jit(solution)/shard_map/all_to_all | solution.py:39
  209.6 0.3 reshape.165
  210.8 0.8 fusion.1
  212.0 14.8 %psum.62 = f32[8,16]{1,0:T(8,128)S(1)} all-reduce(f32[8,16]{1,0:T(8,128)S(1)} %broadcast_multiply_fusion.2), channel_id=1, replica_groups=mesh['tp_0'=8,'tp_1'=8,'dp_0'=4,'dp_1'=2] {'tp_0'}, use_global_device_ids=true, to_apply=%region_21.22 | all-reduce | flops 128 | bytes 1024 | tf_op jit(solution)/shard_map/psum | solution.py:53
  226.7 15.5 %psum.63 = f32[8,16]{1,0:T(8,128)S(1)} all-reduce(f32[8,16]{1,0:T(8,128)S(1)} %psum.62), channel_id=1, replica_groups=mesh['tp_0'=8,'tp_1'=8,'dp_0'=4,'dp_1'=2] {'tp_1'}, use_global_device_ids=true, to_apply=%region_22.23 | all-reduce | flops 128 | bytes 1024 | tf_op jit(solution)/shard_map/psum | solution.py:53
  242.4 0.6 broadcast_in_dim.34
  243.1 3.3 %all-to-all-start.8 = ((bf16[8,8,128]{2,1,0:T(8,128)(2,1)}), bf16[8,8,128]{2,1,0:T(8,128)(2,1)S(1)}, u32[]{:S(2)}, u32[]{:S(2)}) async-start(bf16[8,8,128]{2,1,0:T(8,128)(2,1)} %broadcast_in_dim.34), calls=%async_computation.8 | async-start | bytes 32768 | tf_op jit(solution)/shard_map/all_to_all | solution.py:59
  246.4 0.6 pad_maximum_fusion.1
  247.0 4.7 %all-to-all-done.8 = bf16[8,8,128]{2,1,0:T(8,128)(2,1)S(1)} async-done(((bf16[8,8,128]{2,1,0:T(8,128)(2,1)}), bf16[8,8,128]{2,1,0:T(8,128)(2,1)S(1)}, u32[]{:S(2)}, u32[]{:S(2)}) %all-to-all-start.8) | async-done | bytes 16416 | tf_op jit(solution)/shard_map/all_to_all | solution.py:59
  252.1 0.8 reshape.201
  252.9 7.5 %all-to-all-start.9 = ((f32[64,1,512]{2,1,0:T(1,128)}), f32[64,1,512]{2,1,0:T(1,128)S(1)}, u32[]{:S(2)}, u32[]{:S(2)}) async-start(f32[64,1,512]{2,1,0:T(1,128)} %reshape.201), calls=%async_computation.9 | async-start | bytes 262144 | tf_op jit(solution)/shard_map/all_to_all | solution.py:77
  260.5 0.4 multiply_add_fusion.1
  260.9 11.4 %all-to-all-done.9 = f32[64,1,512]{2,1,0:T(1,128)S(1)} async-done(((f32[64,1,512]{2,1,0:T(1,128)}), f32[64,1,512]{2,1,0:T(1,128)S(1)}, u32[]{:S(2)}, u32[]{:S(2)}) %all-to-all-start.9) | async-done | bytes 131104 | tf_op jit(solution)/shard_map/all_to_all | solution.py:77
  272.3 1.0 reduce.12
  273.5 0.8 reshape.203
  274.3 5.4 %all-to-all-start.10 = ((bf16[64,2,256]{2,1,0:T(2,128)(2,1)}), bf16[64,2,256]{2,1,0:T(2,128)(2,1)S(1)}, u32[]{:S(2)}, u32[]{:S(2)}) async-start(bf16[64,2,256]{2,1,0:T(2,128)(2,1)} %reshape.203), calls=%async_computation.10 | async-start | bytes 131072 | tf_op jit(solution)/shard_map/all_to_all | solution.py:59
  279.7 1.0 pad_maximum_fusion
  280.7 10.5 %all-to-all-done.10 = bf16[64,2,256]{2,1,0:T(2,128)(2,1)S(1)} async-done(((bf16[64,2,256]{2,1,0:T(2,128)(2,1)}), bf16[64,2,256]{2,1,0:T(2,128)(2,1)S(1)}, u32[]{:S(2)}, u32[]{:S(2)}) %all-to-all-start.10) | async-done | bytes 65568 | tf_op jit(solution)/shard_map/all_to_all | solution.py:59
  291.3 0.7 copy.99
  (137 shorter events, 8.5 us)
Async XLA Ops:
  2.3 4.4 %copy-start.14 = (f32[2,2]{1,0:T(2,128)S(1)}, f32[2,2]{1,0:T(2,128)}, u32[]{:S(2)}) copy-start(f32[2,2]{1,0:T(2,128)} %param.31) | copy-start | bytes 52
  2.3 4.5 %copy-start.10 = (f32[2,512]{1,0:T(2,128)S(1)}, f32[2,512]{1,0:T(2,128)}, u32[]{:S(2)}) copy-start(f32[2,512]{1,0:T(2,128)} %param.20) | copy-start | bytes 12292
  2.3 4.5 %copy-start.11 = (bf16[2,4,128]{2,1,0:T(4,128)(2,1)S(1)}, bf16[2,4,128]{2,1,0:T(4,128)(2,1)}, u32[]{:S(2)}) copy-start(bf16[2,4,128]{2,1,0:T(4,128)(2,1)} %param.26) | copy-start | bytes 6148
  2.3 9.6 %all-to-all-start = ((f32[8,64,1]{1,2,0:T(1,128)}), f32[8,64,1]{1,2,0:T(1,128)S(1)}, u32[]{:S(2)}, u32[]{:S(2)}) async-start(f32[8,64,1]{1,2,0:T(1,128)} %broadcast_in_dim.24), calls=%async_computation | async-start | bytes 8192 | tf_op jit(solution)/shard_map/all_to_all | solution.py:59
  6.7 1.4 copy-start.7
  6.8 0.7 copy-start.12
  7.5 0.7 copy-start.13
  8.2 0.7 copy-start.8
  8.2 0.7 copy-start.9
  8.2 0.7 copy-start.16
  8.2 0.7 copy-start.17
  8.2 0.7 copy-start.15
  8.2 3.8 %copy-start.6 = (bf16[2,512,32]{1,2,0:T(8,128)(2,1)S(1)}, bf16[2,512,32]{1,2,0:T(8,128)(2,1)}, u32[]{:S(2)}) copy-start(bf16[2,512,32]{1,2,0:T(8,128)(2,1)} %param.24) | copy-start | bytes 196612
  11.9 0.8 copy-start.5
  12.0 1.2 copy-start.3
  13.0 1.0 copy-start.2
  14.0 0.9 copy-start.4
  16.0 8.9 %all-to-all-start.1 = ((bf16[8,8,448]{2,1,0:T(8,128)(2,1)}), bf16[8,8,448]{2,1,0:T(8,128)(2,1)S(1)}, u32[]{:S(2)}, u32[]{:S(2)}) async-start(bf16[8,8,448]{2,1,0:T(8,128)(2,1)} %bitcast.6), calls=%async_computation.1 | async-start | bytes 131072 | tf_op jit(solution)/shard_map/all_to_all | solution.py:23
  26.1 28.0 %all-to-all-start.2 = ((bf16[64,2,256]{2,1,0:T(2,128)(2,1)}), bf16[64,2,256]{2,1,0:T(2,128)(2,1)S(1)}, u32[]{:S(2)}, u32[]{:S(2)}) async-start(bf16[64,2,256]{2,1,0:T(2,128)(2,1)} %reshape.193), calls=%async_computation.2 | async-start | bytes 131072 | tf_op jit(solution)/shard_map/all_to_all | solution.py:39
  54.2 1.4 copy-start
  55.6 35.5 %copy-start.1 = (bf16[2,128,512]{2,1,0:T(8,128)(2,1)S(1)}, bf16[2,128,512]{2,1,0:T(8,128)(2,1)}, u32[]{:S(2)}) copy-start(bf16[2,128,512]{2,1,0:T(8,128)(2,1)} %param.33) | copy-start | bytes 786436
  87.8 8.6 %all-to-all-start.3 = ((bf16[8,8,128]{2,1,0:T(8,128)(2,1)}), bf16[8,8,128]{2,1,0:T(8,128)(2,1)S(1)}, u32[]{:S(2)}, u32[]{:S(2)}) async-start(bf16[8,8,128]{2,1,0:T(8,128)(2,1)} %broadcast_in_dim.28), calls=%async_computation.3 | async-start | bytes 32768 | tf_op jit(solution)/shard_map/all_to_all | solution.py:59
  97.7 19.4 %all-to-all-start.4 = ((f32[64,1,512]{2,1,0:T(1,128)}), f32[64,1,512]{2,1,0:T(1,128)S(1)}, u32[]{:S(2)}, u32[]{:S(2)}) async-start(f32[64,1,512]{2,1,0:T(1,128)} %reshape.195), calls=%async_computation.4 | async-start | bytes 262144 | tf_op jit(solution)/shard_map/all_to_all | solution.py:77
  161.3 19.0 %all-to-all-start.5 = ((bf16[64,2,256]{2,1,0:T(2,128)(2,1)}), bf16[64,2,256]{2,1,0:T(2,128)(2,1)S(1)}, u32[]{:S(2)}, u32[]{:S(2)}) async-start(bf16[64,2,256]{2,1,0:T(2,128)(2,1)} %reshape.197), calls=%async_computation.5 | async-start | bytes 131072 | tf_op jit(solution)/shard_map/all_to_all | solution.py:59
  182.3 8.9 %all-to-all-start.6 = ((bf16[8,8,448]{2,1,0:T(8,128)(2,1)}), bf16[8,8,448]{2,1,0:T(8,128)(2,1)S(1)}, u32[]{:S(2)}, u32[]{:S(2)}) async-start(bf16[8,8,448]{2,1,0:T(8,128)(2,1)} %bitcast.44), calls=%async_computation.6 | async-start | bytes 131072 | tf_op jit(solution)/shard_map/all_to_all | solution.py:23
  192.4 16.9 %all-to-all-start.7 = ((bf16[64,2,256]{2,1,0:T(2,128)(2,1)}), bf16[64,2,256]{2,1,0:T(2,128)(2,1)S(1)}, u32[]{:S(2)}, u32[]{:S(2)}) async-start(bf16[64,2,256]{2,1,0:T(2,128)(2,1)} %reshape.199), calls=%async_computation.7 | async-start | bytes 131072 | tf_op jit(solution)/shard_map/all_to_all | solution.py:39
  243.1 8.6 %all-to-all-start.8 = ((bf16[8,8,128]{2,1,0:T(8,128)(2,1)}), bf16[8,8,128]{2,1,0:T(8,128)(2,1)S(1)}, u32[]{:S(2)}, u32[]{:S(2)}) async-start(bf16[8,8,128]{2,1,0:T(8,128)(2,1)} %broadcast_in_dim.34), calls=%async_computation.8 | async-start | bytes 32768 | tf_op jit(solution)/shard_map/all_to_all | solution.py:59
  252.9 19.4 %all-to-all-start.9 = ((f32[64,1,512]{2,1,0:T(1,128)}), f32[64,1,512]{2,1,0:T(1,128)S(1)}, u32[]{:S(2)}, u32[]{:S(2)}) async-start(f32[64,1,512]{2,1,0:T(1,128)} %reshape.201), calls=%async_computation.9 | async-start | bytes 262144 | tf_op jit(solution)/shard_map/all_to_all | solution.py:77
  274.3 16.9 %all-to-all-start.10 = ((bf16[64,2,256]{2,1,0:T(2,128)(2,1)}), bf16[64,2,256]{2,1,0:T(2,128)(2,1)S(1)}, u32[]{:S(2)}, u32[]{:S(2)}) async-start(bf16[64,2,256]{2,1,0:T(2,128)(2,1)} %reshape.203), calls=%async_computation.10 | async-start | bytes 131072 | tf_op jit(solution)/shard_map/all_to_all | solution.py:59
